TPU v7x, 32 devices: a whole 2x2x4 slice. The times are simulated.
32 devices in a mesh: sp: 4 (over z), fs: 4 (over y, x), tp: 2 (over core).
Axes of the slice: x: 2, y: 2, z: 4, core: 2. Of those that a mesh axis runs over, the one named last changes fastest.
Arguments:
- tokens: bfloat16 [4, 2048, 2048], P('fs', ('sp', 'tp')), may hold values from -6 to 6
- norm_gain: float32 [2048], replicated, may hold values from 0.1 to 1.9
- query_weight: bfloat16 [2048, 1024], P('sp', 'tp'), may hold values from -20 to 20
- key_matrix: bfloat16 [2048, 256], P('sp', 'tp'), may hold values from -0.125 to 0.125
- value_matrix: bfloat16 [2048, 256], P('sp', 'tp'), may hold values from -0.125 to 0.125
- pool_in_weight: bfloat16 [2048, 1024], P('sp', 'tp'), may hold values from -0.125 to 0.125
- head_sink_logit: float32 [16], replicated, may hold values from 2 to 6
- pool_mix: bfloat16 [4, 256, 256], replicated, may hold values from -0.375 to 0.375
- pool_gain: float32 [1024], replicated, may hold values from 0.1 to 1.9
- attn_out_weight: bfloat16 [1024, 2048], P('tp', 'sp'), may hold values from -1 to 1
- pool_out_weight: bfloat16 [1024, 2048], P('tp', 'sp'), may hold values from -0.125 to 0.125
Outputs:
- mixed: bfloat16 [4, 2048, 2048], P('fs', ('sp', 'tp'))
- row_log_weight_sum: float32 [4, 16, 2048], P('fs', 'tp', 'sp')
All inputs are finite; a program needn't handle non-finite values.
Results may differ from a plain program's by a relative error of at most 0.0095.
The roundings to bfloat16 on the way count: a program that leaves them out, or rounds other values in their place, can miss the bound.
Values may be sent and summed in bfloat16 or wider, within the bound.
A program may use at most 64 MiB of HBM per device.

v0:
```python
import jax
import jax.numpy as jnp
from jax import lax
from jax.sharding import PartitionSpec as P

HEAD_SIZE = 64
WINDOW = 128
POOL_CH = 256


EPSILON = 1e-06
POOL_SPANS = (2, 4, 8, 16)


def passed_along(shard, axis, by):
    size = lax.axis_size(axis)
    pairs = [(i, i + by) for i in range(size) if 0 <= i + by < size]
    return lax.ppermute(shard, axis, pairs)


def windowed_attend(
    query_rows, key_rows, value_rows, key_tail, value_tail, sinks, kv_heads, group, first_pos
):
    rows = query_rows.shape[0]
    blocks = rows // WINDOW
    width = key_rows.shape[1]
    ext_keys = jnp.concatenate([key_tail, key_rows], 0)
    ext_values = jnp.concatenate([value_tail, value_rows], 0)

    def banded(table):
        return jnp.concatenate(
            [
                table[:rows].reshape(blocks, WINDOW, width),
                table[WINDOW:].reshape(blocks, WINDOW, width),
            ],
            axis=1,
        )

    band_keys = banded(ext_keys).reshape(blocks, 2 * WINDOW, kv_heads, HEAD_SIZE)
    band_values = banded(ext_values).reshape(blocks, 2 * WINDOW, kv_heads, HEAD_SIZE)
    query_blocks = query_rows.reshape(blocks, WINDOW, kv_heads, group, HEAD_SIZE)
    scores = jnp.einsum(
        "bqkgd,bskd->bkgqs", query_blocks, band_keys, preferred_element_type=jnp.float32
    ) * HEAD_SIZE ** (-0.5)
    query_pos = first_pos + jnp.arange(rows).reshape(blocks, WINDOW, 1)
    key_pos = (
        first_pos
        - WINDOW
        + jnp.arange(blocks).reshape(blocks, 1, 1) * WINDOW
        + jnp.arange(2 * WINDOW).reshape(1, 1, 2 * WINDOW)
    )
    offset = query_pos - key_pos
    allowed = (offset >= 0) & (offset < WINDOW) & (key_pos >= 0)
    scores = jnp.where(allowed[:, None, None], scores, -jnp.inf)
    sink_grid = sinks.reshape(1, kv_heads, group, 1, 1)
    top = jnp.maximum(jnp.max(scores, axis=-1, keepdims=True), sink_grid)
    weights = jnp.exp(scores - top)
    total = jnp.sum(weights, axis=-1, keepdims=True) + jnp.exp(sink_grid - top)
    probs = (weights / total).astype(jnp.bfloat16)
    mixed = jnp.einsum(
        "bkgqs,bskd->bqkgd", probs, band_values, preferred_element_type=jnp.float32
    ).astype(jnp.bfloat16)
    row_log_weight_sum = (top + jnp.log(total))[..., 0]
    return (
        mixed.reshape(rows, kv_heads * group * HEAD_SIZE),
        row_log_weight_sum.transpose(1, 2, 0, 3).reshape(kv_heads * group, rows),
    )


def pool_branch(pool_rows, pool_tail, mixing, scales, group_start, first_pos):
    rows = pool_rows.shape[0]
    columns = pool_rows.shape[1]
    pool_reach = max(POOL_SPANS)
    extended = jnp.concatenate([pool_tail, pool_rows], 0).astype(jnp.float32)
    group_index = group_start + jnp.arange(columns) // POOL_CH
    span_table = jnp.array(POOL_SPANS, jnp.int32)
    matches = group_index[:, None] == jnp.arange(len(POOL_SPANS))[None, :]
    span_of_col = jnp.sum(jnp.where(matches, span_table[None, :], 0), axis=1)
    trailing = jnp.zeros((rows, columns), jnp.float32)
    for lag in range(pool_reach):
        trailing = trailing + jnp.where(
            lag < span_of_col[None, :], extended[pool_reach - lag : pool_reach - lag + rows], 0.0
        )
    position = first_pos + jnp.arange(rows)
    count = jnp.minimum(position[:, None] + 1, span_of_col[None, :]).astype(jnp.float32)
    centred = (trailing / count - extended[pool_reach:]).astype(jnp.bfloat16)
    grouped = centred.reshape(rows, columns // POOL_CH, POOL_CH)
    product = jnp.einsum(
        "rgc,gcd->rgd", grouped, mixing, preferred_element_type=jnp.float32
    ).reshape(rows, columns)
    return (product * scales).astype(jnp.bfloat16)


def local(
    tokens,
    norm_gain,
    query_weight,
    key_matrix,
    value_matrix,
    pool_in_weight,
    head_sink_logit,
    pool_mix,
    pool_gain,
    attn_out_weight,
    pool_out_weight,
):
    tp_index = lax.axis_index("tp")
    sp_index = lax.axis_index("sp")
    q_cols = query_weight.shape[1]
    kv_cols = key_matrix.shape[1]
    pool_cols = pool_in_weight.shape[1]
    q_heads = q_cols // HEAD_SIZE
    kv_heads = kv_cols // HEAD_SIZE
    groups_dev = pool_cols // POOL_CH
    full_query, full_key, full_value, full_pool = (
        lax.all_gather(query_weight, "sp", axis=0, tiled=True),
        lax.all_gather(key_matrix, "sp", axis=0, tiled=True),
        lax.all_gather(value_matrix, "sp", axis=0, tiled=True),
        lax.all_gather(pool_in_weight, "sp", axis=0, tiled=True),
    )
    values_f = lax.all_gather(tokens[0], "tp", axis=0, tiled=True).astype(jnp.float32)
    scale = lax.rsqrt(jnp.mean(values_f * values_f, axis=-1, keepdims=True) + EPSILON)
    normed = (values_f * scale * norm_gain).astype(jnp.bfloat16)
    outputs = [
        jnp.dot(normed, weight, preferred_element_type=jnp.float32).astype(jnp.bfloat16)
        for weight in (full_query, full_key, full_value, full_pool)
    ]
    projected = jnp.concatenate(outputs, axis=1)
    rows = projected.shape[0]
    first_pos = sp_index * rows
    query_rows = projected[:, :q_cols]
    key_rows = projected[:, q_cols : q_cols + kv_cols]
    value_rows = projected[:, q_cols + kv_cols : q_cols + 2 * kv_cols]
    pool_rows = projected[:, q_cols + 2 * kv_cols :]
    pool_reach = max(POOL_SPANS)
    sinks = lax.dynamic_slice_in_dim(head_sink_logit, tp_index * q_heads, q_heads, 0)
    mixing = lax.dynamic_slice_in_dim(pool_mix, tp_index * groups_dev, groups_dev, 0)
    scales = lax.dynamic_slice_in_dim(pool_gain, tp_index * pool_cols, pool_cols, 0)
    key_tail, value_tail, pool_tail = passed_along(
        (key_rows[rows - WINDOW :], value_rows[rows - WINDOW :], pool_rows[rows - pool_reach :]),
        "sp",
        1,
    )
    attn_part, log_part = windowed_attend(
        query_rows,
        key_rows,
        value_rows,
        key_tail,
        value_tail,
        sinks,
        kv_heads,
        q_heads // kv_heads,
        first_pos,
    )
    pool_part = pool_branch(pool_rows, pool_tail, mixing, scales, tp_index * groups_dev, first_pos)
    half_attn, half_pool = (
        lax.all_gather(attn_out_weight, "sp", axis=1, tiled=True),
        lax.all_gather(pool_out_weight, "sp", axis=1, tiled=True),
    )
    result = lax.psum_scatter(
        jnp.dot(attn_part, half_attn, preferred_element_type=jnp.float32)
        + jnp.dot(pool_part, half_pool, preferred_element_type=jnp.float32),
        "tp",
        scatter_dimension=0,
        tiled=True,
    ).astype(jnp.bfloat16)
    return (result[None], log_part[None])


def solution(mesh):
    in_specs = (
        P("fs", ("sp", "tp"), None),
        P(),
        P("sp", "tp"),
        P("sp", "tp"),
        P("sp", "tp"),
        P("sp", "tp"),
        P(),
        P(),
        P(),
        P("tp", "sp"),
        P("tp", "sp"),
    )
    out_specs = (P("fs", ("sp", "tp"), None), P("fs", "tp", "sp"))
    return jax.shard_map(local, mesh=mesh, in_specs=in_specs, out_specs=out_specs, check_vma=False)
```

profile of v0, /device:TPU:0, one launch (start us, length us, event | category | flops | bytes accessed | tf_op | source)
XLA Modules:
  0.0 243.1 jit_solution(15689682092924149541)
XLA Ops:
  7.3 0.7 all-gather.15.cloned.1.call-update
  8.0 0.7 all-gather.7.cloned.1.call-update
  8.7 0.7 all-gather.11.cloned.1.call-update
  9.5 0.5 all-gather.9.cloned.1.call-update
  10.1 0.5 all-gather.13.cloned.1.call-update
  10.8 17.6 %all_gather.23 = bf16[2048,128]{1,0:T(8,128)(2,1)S(1)} all-gather(bf16[512,128]{1,0:T(8,128)(2,1)} %param.15), channel_id=1, replica_groups=mesh['sp'=4,'fs'=4,'tp'=2] {'sp'}, dimensions={0}, use_global_device_ids=true | all-gather | bytes 655360 | tf_op jit(solution)/shard_map/all_gather | solution.py:117
  28.4 0.7 dynamic_slice.9
  29.2 23.4 %all_gather.22 = bf16[2048,128]{1,0:T(8,128)(2,1)} all-gather(bf16[512,128]{1,0:T(8,128)(2,1)} %param.16), channel_id=1, replica_groups=mesh['sp'=4,'fs'=4,'tp'=2] {'sp'}, dimensions={0}, use_global_device_ids=true | all-gather | bytes 655360 | tf_op jit(solution)/shard_map/all_gather | solution.py:118
  52.7 0.6 broadcast_compare_fusion.15
  53.5 0.3 fusion.36
  53.9 2.2 fusion
  56.1 2.4 convolution_convert_fusion.2
  58.5 0.6 slice.86
  59.1 3.5 %collective-permute-start.1 = (bf16[128,128]{1,0:T(8,128)(2,1)}, bf16[128,128]{1,0:T(8,128)(2,1)}, u32[]{:S(2)}, u32[]{:S(2)}) collective-permute-start(bf16[128,128]{1,0:T(8,128)(2,1)} %slice.86), channel_id=1, source_target_pairs={{0,8},{8,16},{16,24},{1,9},{9,17},{17,25},{2,10},{10,18},{18,26},{... | collective-permute-start | bytes 98312 | tf_op jit(solution)/shard_map/ppermute | solution.py:18
  62.6 1.5 convolution_convert_fusion.3
  64.1 0.1 reshape.235
  64.2 0.6 slice.85
  64.8 0.1 reshape.233
  65.0 0.8 copy.45
  65.8 2.0 collective-permute-start
  67.8 0.8 copy.41
  68.5 0.8 pad_maximum_fusion
  69.3 0.1 reshape.234
  69.5 0.8 copy.44
  70.3 0.1 reshape.232
  70.5 0.8 copy.40
  71.3 5.5 %all-gather.7.cloned.1.call-done = bf16[2048,512]{1,0:T(8,128)(2,1)} async-done(((bf16[512,512]{1,0:T(8,128)(2,1)}), bf16[2048,512]{1,0:T(8,128)(2,1)}) %all-gather.7.cloned.1.call-update) | async-done | bytes 2097168 | tf_op jit(solution)/shard_map/all_gather | solution.py:116
  76.8 2.9 %convolution_convert_fusion.1 = bf16[512,512]{1,0:T(8,128)(2,1)S(1)} fusion(bf16[2048,512]{1,0:T(8,128)(2,1)} %all-gather.7.cloned.1.call-done, bf16[1,512,2048]{2,1,0:T(8,128)(2,1)S(1)} %copy-done.1, f32[2048]{0:T(1024)} %param.13, f32[512]{0:T(512)} %copy-done.23), kind=kOutput, calls=%fused_computation.13 | convolution fusion | flops 1078198272 | bytes 4728832 | tf_op jit(solution)/shard_map/dot_general | solution.py:125
  79.7 1.5 reshape.236
  81.3 2.3 fusion.4
  83.6 1.0 fusion.3
  84.7 1.2 fusion.7
  85.9 0.4 copy.49
  86.3 38.3 %all-gather.11.cloned.1.call-done = bf16[2048,512]{1,0:T(8,128)(2,1)} async-done(((bf16[512,512]{1,0:T(8,128)(2,1)}), bf16[2048,512]{1,0:T(8,128)(2,1)}) %all-gather.11.cloned.1.call-update) | async-done | bytes 2097168 | tf_op jit(solution)/shard_map/all_gather | solution.py:119
  124.6 2.9 %convolution_convert_fusion = bf16[512,512]{1,0:T(8,128)(2,1)S(1)} fusion(bf16[2048,512]{1,0:T(8,128)(2,1)} %all-gather.11.cloned.1.call-done, bf16[1,512,2048]{2,1,0:T(8,128)(2,1)S(1)} %copy-done.1, f32[2048]{0:T(1024)S(1)} %copy-done.28, f32[512]{0:T(512)S(1)} %copy-done.24), kind=kOutput, calls=%fused_computation.12 | convolution fusion | flops 1078198272 | bytes 4728832 | tf_op jit(solution)/shard_map/dot_general | solution.py:125
  127.5 0.8 copy-done.2
  128.3 2.4 collective-permute-start.2
  130.7 39.8 %all-gather.9.cloned.1.call-done = bf16[512,2048]{1,0:T(8,128)(2,1)} async-done(((bf16[512,512]{1,0:T(8,128)(2,1)}), bf16[512,2048]{1,0:T(8,128)(2,1)}) %all-gather.9.cloned.1.call-update) | async-done | bytes 2097168 | tf_op jit(solution)/shard_map/all_gather | solution.py:157
  170.6 4.9 %fusion.29 = f32[512,2048]{1,0:T(8,128)} fusion(bf16[512,2048]{1,0:T(8,128)(2,1)} %all-gather.9.cloned.1.call-done, bf16[64,8,4,128]{3,2,1,0:T(4,128)(2,1)S(1)} %bitcast.76), kind=kOutput, calls=%fused_computation.59 | convolution fusion | flops 1073741824 | bytes 6815744 | tf_op jit(solution)/shard_map/dot_general | solution.py:161
  175.5 0.1 maximum_convert_fusion
  175.8 3.0 %fusion.28 = bf16[512,512]{1,0:T(8,128)(2,1)S(1)} fusion(f32[528,512]{1,0:T(8,128)S(1)} %maximum_convert_fusion, s32[512]{0:T(512)S(1)} %select_reduce_fusion, s32[512]{0:T(512)S(1)} %add_add_fusion, pred[512]{0:T(512)(128)(4,1)S(1)} %copy-done.8, pred[512]{0:T(512)(128)(4,1)S(1)} %copy-done.9, pred[512]{0:T(512)(128)(4,1)S(1)} %copy-done.10, ...), kind=kLoop, calls=%fused_computation.55 | loop fusion | flops 9437184 | bytes 17313792 | tf_op jit(solution)/shard_map/convert_element_type | solution.py:86
  178.8 0.4 fusion.32
  179.2 0.1 fusion.25
  179.3 37.1 %all-gather.13.cloned.1.call-done = bf16[512,2048]{1,0:T(8,128)(2,1)} async-done(((bf16[512,512]{1,0:T(8,128)(2,1)}), bf16[512,2048]{1,0:T(8,128)(2,1)}) %all-gather.13.cloned.1.call-update) | async-done | bytes 2097168 | tf_op jit(solution)/shard_map/all_gather | solution.py:158
  216.4 6.1 %convolution_add_fusion = f32[512,2048]{1,0:T(8,128)} fusion(f32[512,2048]{1,0:T(8,128)} %fusion.29, bf16[512,512]{0,1:T(8,128)(2,1)S(1)} %fusion.25, bf16[512,2048]{1,0:T(8,128)(2,1)} %all-gather.13.cloned.1.call-done), kind=kOutput, calls=%fused_computation.9 | convolution fusion | flops 1074790400 | bytes 11010048 | tf_op jit(solution)/shard_map/dot_general | solution.py:162
  222.5 0.7 fusion.43
  223.2 10.3 %reduce-scatter.2.cloned.1.call-done = f32[256,2048]{1,0:T(8,128)} async-done(((f32[512,2048]{1,0:T(8,128)}), f32[256,2048]{1,0:T(8,128)}) %reduce-scatter.2.cloned.1.call-update) | async-done | bytes 2097168 | tf_op jit(solution)/shard_map/reduce_scatter | solution.py:160
  233.5 2.7 %convert_bitcast_fusion = bf16[1,256,2048]{2,1,0:T(8,128)(2,1)} fusion(f32[256,2048]{1,0:T(8,128)} %reduce-scatter.2.cloned.1.call-done), kind=kLoop, calls=%fused_computation.54 | loop fusion | flops 524288 | bytes 3145728 | tf_op jit(solution)/shard_map/broadcast_in_dim | solution.py:167
  (82 shorter events, 1.1 us)
Async XLA Ops:
  7.2 171.7 %copy-start = (bf16[4,256,256]{2,1,0:T(8,128)(2,1)S(1)}, bf16[4,256,256]{2,1,0:T(8,128)(2,1)}, u32[]{:S(2)}) copy-start(bf16[4,256,256]{2,1,0:T(8,128)(2,1)} %param.19) | copy-start | bytes 1572868
  7.2 45.5 %copy-start.26 = (s32[4]{0:T(128)S(1)}, s32[4]{0:T(128)}, u32[]{:S(2)}) copy-start(s32[4]{0:T(128)} %constant.89.clone) | copy-start | bytes 52
  7.2 46.2 %copy-start.25 = (f32[1024]{0:T(1024)S(1)}, f32[1024]{0:T(1024)}, u32[]{:S(2)}) copy-start(f32[1024]{0:T(1024)} %param.20) | copy-start | bytes 12292
  7.2 48.9 %copy-start.27 = (f32[2048]{0:T(1024)S(1)}, f32[2048]{0:T(1024)}, u32[]{:S(2)}) copy-start(f32[2048]{0:T(1024)} %param.13) | copy-start | bytes 24580
  7.2 46.6 %all-gather.15.cloned.1.call-start = ((), (), s32[]{:S(2)}) async-start(), calls=%async_computation.6 | async-start | bytes 3145728 | tf_op jit(solution)/shard_map/all_gather | solution.py:121
  7.9 68.9 %all-gather.7.cloned.1.call-start = ((), (), s32[]{:S(2)}) async-start(), calls=%async_computation.1 | async-start | bytes 2621440 | tf_op jit(solution)/shard_map/all_gather | solution.py:116
  8.7 115.9 %all-gather.11.cloned.1.call-start = ((), (), s32[]{:S(2)}) async-start(), calls=%async_computation.3 | async-start | bytes 2621440 | tf_op jit(solution)/shard_map/all_gather | solution.py:119
  9.4 161.1 %all-gather.9.cloned.1.call-start = ((), (), s32[]{:S(2)}) async-start(), calls=%async_computation.2 | async-start | bytes 2621440 | tf_op jit(solution)/shard_map/all_gather | solution.py:157
  10.0 206.4 %all-gather.13.cloned.1.call-start = ((), (), s32[]{:S(2)}) async-start(), calls=%async_computation.4 | async-start | bytes 2621440 | tf_op jit(solution)/shard_map/all_gather | solution.py:158
  10.6 222.9 %reduce-scatter.2.cloned.1.call-start = ((), (), s32[]{:S(2)}) async-start(), calls=%async_computation.5 | async-start | bytes 6291456 | tf_op jit(solution)/shard_map/reduce_scatter | solution.py:160
  53.8 8.8 %copy-start.1 = (bf16[1,512,2048]{2,1,0:T(8,128)(2,1)S(1)}, bf16[1,512,2048]{2,1,0:T(8,128)(2,1)}, u32[]{:S(2)}) copy-start(bf16[1,512,2048]{2,1,0:T(8,128)(2,1)} %all-gather.15.cloned.1.call-done) | copy-start | bytes 6291460
  53.8 8.8 %copy-start.4 = (bf16[2048,128]{1,0:T(8,128)(2,1)S(1)}, bf16[2048,128]{1,0:T(8,128)(2,1)}, u32[]{:S(2)}) copy-start(bf16[2048,128]{1,0:T(8,128)(2,1)} %all_gather.22) | copy-start | bytes 1572868
  56.1 6.5 %copy-start.23 = (f32[512]{0:T(512)}, f32[512]{0:T(512)S(1)}, u32[]{:S(2)}) copy-start(f32[512]{0:T(512)S(1)} %add_rsqrt_fusion) | copy-start | bytes 6148
  59.1 9.4 %collective-permute-start.1 = (bf16[128,128]{1,0:T(8,128)(2,1)}, bf16[128,128]{1,0:T(8,128)(2,1)}, u32[]{:S(2)}, u32[]{:S(2)}) collective-permute-start(bf16[128,128]{1,0:T(8,128)(2,1)} %slice.86), channel_id=1, source_target_pairs={{0,8},{8,16},{16,24},{1,9},{9,17},{17,25},{2,10},{10,18},{18,26},{... | collective-permute-start | bytes 98312 | tf_op jit(solution)/shard_map/ppermute | solution.py:18
  65.8 4.6 %collective-permute-start = (bf16[128,128]{1,0:T(8,128)(2,1)}, bf16[128,128]{1,0:T(8,128)(2,1)S(1)}, u32[]{:S(2)}, u32[]{:S(2)}) collective-permute-start(bf16[128,128]{1,0:T(8,128)(2,1)} %slice.85), channel_id=1, source_target_pairs={{0,8},{8,16},{16,24},{1,9},{9,17},{17,25},{2,10},{10,18},{18,26},{... | collective-permute-start | bytes 98312 | tf_op jit(solution)/shard_map/ppermute | solution.py:18
  81.2 3.4 %copy-start.5 = (bf16[4,128,2,64]{1,3,2,0:T(8,128)(2,1)S(1)}, bf16[4,128,2,64]{1,3,2,0:T(8,128)(2,1)}, u32[]{:S(2)}) copy-start(bf16[4,128,2,64]{1,3,2,0:T(8,128)(2,1)} %copy.41) | copy-start | bytes 393220
  81.2 3.4 %copy-start.6 = (bf16[4,128,2,64]{1,3,2,0:T(8,128)(2,1)S(1)}, bf16[4,128,2,64]{1,3,2,0:T(8,128)(2,1)}, u32[]{:S(2)}) copy-start(bf16[4,128,2,64]{1,3,2,0:T(8,128)(2,1)} %copy.40) | copy-start | bytes 393220
  84.7 39.9 %copy-start.24 = (f32[512]{0:T(512)S(1)}, f32[512]{0:T(512)}, u32[]{:S(2)}) copy-start(f32[512]{0:T(512)} %copy-done.23) | copy-start | bytes 6148
  84.7 39.9 %copy-start.28 = (f32[2048]{0:T(1024)S(1)}, f32[2048]{0:T(1024)}, u32[]{:S(2)}) copy-start(f32[2048]{0:T(1024)} %param.13) | copy-start | bytes 24580
  127.5 0.8 copy-start.2
  128.3 47.2 %copy-start.3 = (bf16[512,512]{1,0:T(8,128)(2,1)S(1)}, bf16[512,512]{1,0:T(8,128)(2,1)}, u32[]{:S(2)}) copy-start(bf16[512,512]{1,0:T(8,128)(2,1)} %copy-done.2) | copy-start | bytes 1572868
  128.3 47.2 %collective-permute-start.2 = (bf16[16,512]{1,0:T(8,128)(2,1)S(1)}, bf16[16,512]{1,0:T(8,128)(2,1)S(1)}, u32[]{:S(2)}, u32[]{:S(2)}) collective-permute-start(bf16[16,512]{1,0:T(8,128)(2,1)S(1)} %slice.87), channel_id=1, source_target_pairs={{0,8},{8,16},{16,24},{1,9},{9,17},{17,25},{2,10},{10,18},{18,26},{... | collective-permute-start | bytes 49160 | tf_op jit(solution)/shard_map/ppermute | solution.py:18
  170.5 5.1 %copy-start.7 = (pred[512]{0:T(512)(128)(4,1)S(1)}, pred[512]{0:T(512)(128)(4,1)}, u32[]{:S(2)}) copy-start(pred[512]{0:T(512)(128)(4,1)} %get-tuple-element.2) | copy-start | bytes 1540
  170.5 5.1 %copy-start.8 = (pred[512]{0:T(512)(128)(4,1)S(1)}, pred[512]{0:T(512)(128)(4,1)}, u32[]{:S(2)}) copy-start(pred[512]{0:T(512)(128)(4,1)} %get-tuple-element.3) | copy-start | bytes 1540
  170.5 5.1 %copy-start.9 = (pred[512]{0:T(512)(128)(4,1)S(1)}, pred[512]{0:T(512)(128)(4,1)}, u32[]{:S(2)}) copy-start(pred[512]{0:T(512)(128)(4,1)} %get-tuple-element.4) | copy-start | bytes 1540
  170.5 5.1 %copy-start.10 = (pred[512]{0:T(512)(128)(4,1)S(1)}, pred[512]{0:T(512)(128)(4,1)}, u32[]{:S(2)}) copy-start(pred[512]{0:T(512)(128)(4,1)} %get-tuple-element.5) | copy-start | bytes 1540
  170.5 5.1 %copy-start.11 = (pred[512]{0:T(512)(128)(4,1)S(1)}, pred[512]{0:T(512)(128)(4,1)}, u32[]{:S(2)}) copy-start(pred[512]{0:T(512)(128)(4,1)} %get-tuple-element.6) | copy-start | bytes 1540
  170.5 5.2 %copy-start.12 = (pred[512]{0:T(512)(128)(4,1)S(1)}, pred[512]{0:T(512)(128)(4,1)}, u32[]{:S(2)}) copy-start(pred[512]{0:T(512)(128)(4,1)} %get-tuple-element.7) | copy-start | bytes 1540
  170.5 5.2 %copy-start.13 = (pred[512]{0:T(512)(128)(4,1)S(1)}, pred[512]{0:T(512)(128)(4,1)}, u32[]{:S(2)}) copy-start(pred[512]{0:T(512)(128)(4,1)} %get-tuple-element.8) | copy-start | bytes 1540
  170.6 5.2 %copy-start.14 = (pred[512]{0:T(512)(128)(4,1)S(1)}, pred[512]{0:T(512)(128)(4,1)}, u32[]{:S(2)}) copy-start(pred[512]{0:T(512)(128)(4,1)} %get-tuple-element.9) | copy-start | bytes 1540
  170.6 5.2 %copy-start.15 = (pred[512]{0:T(512)(128)(4,1)S(1)}, pred[512]{0:T(512)(128)(4,1)}, u32[]{:S(2)}) copy-start(pred[512]{0:T(512)(128)(4,1)} %get-tuple-element.10) | copy-start | bytes 1540
  170.6 5.2 %copy-start.16 = (pred[512]{0:T(512)(128)(4,1)S(1)}, pred[512]{0:T(512)(128)(4,1)}, u32[]{:S(2)}) copy-start(pred[512]{0:T(512)(128)(4,1)} %get-tuple-element.11) | copy-start | bytes 1540
  170.6 5.2 %copy-start.17 = (pred[512]{0:T(512)(128)(4,1)S(1)}, pred[512]{0:T(512)(128)(4,1)}, u32[]{:S(2)}) copy-start(pred[512]{0:T(512)(128)(4,1)} %get-tuple-element.12) | copy-start | bytes 1540
  170.6 5.2 %copy-start.18 = (pred[512]{0:T(512)(128)(4,1)S(1)}, pred[512]{0:T(512)(128)(4,1)}, u32[]{:S(2)}) copy-start(pred[512]{0:T(512)(128)(4,1)} %get-tuple-element.13) | copy-start | bytes 1540
  170.6 5.2 %copy-start.19 = (pred[512]{0:T(512)(128)(4,1)S(1)}, pred[512]{0:T(512)(128)(4,1)}, u32[]{:S(2)}) copy-start(pred[512]{0:T(512)(128)(4,1)} %get-tuple-element.14) | copy-start | bytes 1540
  170.6 5.2 %copy-start.20 = (pred[512]{0:T(512)(128)(4,1)S(1)}, pred[512]{0:T(512)(128)(4,1)}, u32[]{:S(2)}) copy-start(pred[512]{0:T(512)(128)(4,1)} %get-tuple-element.15) | copy-start | bytes 1540
  170.6 5.2 %copy-start.21 = (pred[512]{0:T(512)(128)(4,1)S(1)}, pred[512]{0:T(512)(128)(4,1)}, u32[]{:S(2)}) copy-start(pred[512]{0:T(512)(128)(4,1)} %get-tuple-element.16) | copy-start | bytes 1540
  170.6 5.2 %copy-start.22 = (pred[512]{0:T(512)(128)(4,1)S(1)}, pred[512]{0:T(512)(128)(4,1)}, u32[]{:S(2)}) copy-start(pred[512]{0:T(512)(128)(4,1)} %get-tuple-element.17) | copy-start | bytes 1540
Sparse Core Ops, SparseCore 0:
  9.6 13.2 all-gather.14
  24.5 52.2 all-gather.6
  78.4 46.1 all-gather.10
  126.0 44.4 all-gather.8
  171.9 44.4 all-gather.12
  222.7 10.8 reduce-scatter.1
where the time goes:
time: 244 us; the launch traced here: 243 us
  waiting for transfers between devices  134 us (55%)
  blocking collectives  41 us (17%)
  matrix products  24.4 us (10%)
  between operations  14.6 us (6%)
  other arithmetic  12.1 us (5%)
  local copies, waits for them, and re-layouts  8.64 us (4%)
  starting transfers between devices  8.09 us (3%)
    all_gather x1, waiting for transfers between devices, local(): lax.all_gather(attn_out_weight, 'sp', axis=1, tiled=True)  39.8 us
    all_gather x1, waiting for transfers between devices, local(): lax.all_gather(pool_in_weight, 'sp', axis=0, tiled=True)  38.3 us
    all_gather x1, waiting for transfers between devices, local(): lax.all_gather(pool_out_weight, 'sp', axis=1, tiled=True)  37.1 us
    all_gather x1, blocking collectives, local(): lax.all_gather(value_matrix, 'sp', axis=0, tiled=True)  23.4 us
    all_gather x1, blocking collectives, local(): lax.all_gather(key_matrix, 'sp', axis=0, tiled=True)  17.6 us
    reduce_scatter x1, waiting for transfers between devices, local(): lax.psum_scatter(jnp.dot(attn_part, half_attn, preferred_element_type=jnp...  10.3 us
    dot_general x4, matrix products, local(): jnp.dot(normed, weight, preferred_element_type=jnp.float32)  9.63 us
    ppermute x3, starting transfers between devices, passed_along(): return lax.ppermute(shard, axis, pairs)  7.87 us
  transfers between devices with their start and end apart: 9, of which 6 were waited for; matrix products, arithmetic and copies ran while one was open for 15% of the time, Pallas kernels for 0%

commit v1 on v0

--- a/solution.py
+++ b/solution.py
@@ -1,6 +1,10 @@
+import functools
+
 import jax
 import jax.numpy as jnp
 from jax import lax
+from jax.experimental import pallas as pl
+from jax.experimental.pallas import tpu as pltpu
 from jax.sharding import PartitionSpec as P
 
 HEAD_SIZE = 64
@@ -167,6 +171,508 @@
     return (result[None], log_part[None])
 
 
+LANES = 128
+TILE = 16
+MESH_ID = pl.DeviceIdType.MESH
+
+
+def nearest(n, step, me):
+    tables = [sorted((j for j in range(n) if j != z), key=lambda j: (abs(j - z), j)) for z in range(n)]
+    shard = jnp.int32(tables[0][step])
+    for z in range(1, n):
+        shard = jnp.where(me == z, tables[z][step], shard)
+    return shard
+
+
+def layer_kernel(
+    n,
+    sinks,
+    tokens,
+    gain,
+    wq,
+    wk,
+    wv,
+    wp,
+    mix,
+    pool_gain,
+    wao,
+    wpo,
+    out,
+    log_out,
+    held,
+    tok,
+    normed,
+    proj,
+    kv,
+    pool_ext,
+    mixed,
+    mix_own,
+    mine,
+    sent,
+    got,
+    z_send,
+    x_send,
+    y_send,
+    z_recv,
+    x_recv,
+    y_recv,
+    load_sem,
+    tok_sem,
+    halo_send,
+    halo_recv,
+    sum_send,
+    sum_recv,
+):
+    me = lax.axis_index("sp")
+    f = lax.axis_index("fs")
+    c = lax.axis_index("tp")
+    f32 = jnp.float32
+    half = tokens.shape[0]
+    rows = 2 * half
+    depth = wq.shape[0]
+    n_in = (wq.shape[1] + wk.shape[1] + wv.shape[1] + wp.shape[1]) // LANES
+    out_tiles = wao.shape[1] // LANES
+    n_blocks = n_in + 2 * out_tiles
+    steps = n_blocks // 3
+    sources = [wk, wv] + [wq.at[:, pl.ds(i * LANES, LANES)] for i in range(wq.shape[1] // LANES)]
+    sources += [wp.at[:, pl.ds(i * LANES, LANES)] for i in range(wp.shape[1] // LANES)]
+    for i in range(out_tiles):
+        sources += [w.at[:, pl.ds(i * LANES, LANES)] for w in (wao, wpo)]
+    z_part = lax.rem(f, 3)
+    beside = f + 1 - 2 * lax.rem(f, 2)
+    across = lax.rem(f + 2, 4)
+    x_part = lax.rem(beside, 3)
+    y_part = 3 - z_part - x_part
+    relays = (f == 0) | (f == 3)
+    y_out = jnp.where(relays, x_part, z_part)
+    up, down = me + 1, me - 1
+    has_up, has_down = me < n - 1, me > 0
+
+    def load(i):
+        return pltpu.make_async_copy(sources[i], held.at[me, i], load_sem.at[i])
+
+    for i in range(n_blocks):
+        load(i).start()
+    own_rows = pl.ds(pl.multiple_of(c * half, half), half)
+    tok_load = pltpu.make_async_copy(tokens, tok.at[own_rows], tok_sem.at[2])
+    tok_load.start()
+    groups = mix_own.shape[0]
+    mix_load = pltpu.make_async_copy(mix.at[pl.ds(c * groups, groups)], mix_own, tok_sem.at[3])
+    mix_load.start()
+
+    barrier = pltpu.get_barrier_semaphore()
+    pl.semaphore_signal(barrier, inc=1, device_id={"tp": 1 - c}, device_id_type=MESH_ID)
+    pl.semaphore_signal(barrier, inc=1, device_id={"fs": beside}, device_id_type=MESH_ID)
+    pl.semaphore_signal(barrier, inc=1, device_id={"fs": across}, device_id_type=MESH_ID)
+
+    @pl.when(has_up)
+    def _():
+        pl.semaphore_signal(barrier, inc=1, device_id={"sp": up}, device_id_type=MESH_ID)
+
+    @pl.when(has_down)
+    def _():
+        pl.semaphore_signal(barrier, inc=1, device_id={"sp": down}, device_id_type=MESH_ID)
+
+    pl.semaphore_wait(barrier, 3 + has_up.astype(jnp.int32) + has_down.astype(jnp.int32))
+
+    tok_send = pltpu.make_async_remote_copy(
+        tokens, tok.at[own_rows], tok_sem.at[0], tok_sem.at[1],
+        device_id={"tp": 1 - c}, device_id_type=MESH_ID,
+    )
+    tok_send.start()
+
+    def hop(s, j, part, send, recv, to):
+        block = held.at[j, 3 * s + part]
+        return pltpu.make_async_remote_copy(
+            block, block, send, recv.at[s, j], device_id=to, device_id_type=MESH_ID
+        )
+
+    def z_hop(s, j, way):
+        to = jnp.where(way == 0, up, down)
+        return hop(s, j, z_part, z_send.at[way, s, j], z_recv, {"sp": to})
+
+    def x_hop(s, j):
+        return hop(s, j, z_part, x_send.at[s, j], x_recv, {"fs": beside})
+
+    def y_hop(s, j):
+        return hop(s, j, y_out, y_send.at[s, j], y_recv, {"fs": across})
+
+    def onward(j):
+        return jnp.where(j < me, 0, 1), ((j < me) & has_up) | ((j > me) & has_down)
+
+    def own_send(s, finish=False):
+        @pl.when(has_up)
+        def _():
+            cp = z_hop(s, me, 0)
+            cp.wait_send() if finish else cp.start()
+
+        @pl.when(has_down)
+        def _():
+            cp = z_hop(s, me, 1)
+            cp.wait_send() if finish else cp.start()
+
+    slots = [(s, k) for s in range(steps) for k in range(n - 1)]
+    shard = [nearest(n, k, me) for k in range(n - 1)]
+
+    def z_step(t):
+        s, k = slots[t]
+        j = shard[k]
+        if k == 0 and s + 1 < steps:
+            own_send(s + 1)
+        z_hop(s, j, 0).wait_recv()
+        way, more = onward(j)
+
+        @pl.when(more)
+        def _():
+            z_hop(s, j, way).start()
+
+        x_hop(s, j).start()
+
+    def x_step(t):
+        s, k = slots[t]
+        hop(s, shard[k], x_part, x_send.at[s, shard[k]], x_recv, {"fs": beside}).wait_recv()
+        y_hop(s, shard[k]).start()
+
+    def y_step(t):
+        s, k = slots[t]
+        hop(s, shard[k], y_part, y_send.at[s, shard[k]], y_recv, {"fs": across}).wait_recv()
+
+    for i in range(n_blocks):
+        load(i).wait()
+        if i % 3 == 2 and i // 3 == 0:
+            own_send(0)
+
+    def norm_rows(r, size):
+        v = tok[pl.ds(r, size), :].astype(f32)
+        scale = lax.rsqrt(jnp.mean(v * v, axis=-1, keepdims=True) + EPSILON)
+        normed[pl.ds(r, size), :] = (v * scale * gain[...]).astype(jnp.bfloat16)
+
+    def norm_all():
+        tok_load.wait()
+        tok_send.wait()
+        mix_load.wait()
+        chunk = 32
+
+        @pl.loop(0, rows // chunk)
+        def _(i):
+            norm_rows(pl.multiple_of(i * chunk, chunk), chunk)
+
+    def project(pair):
+        acc = None
+        for j in range(n):
+            w = jnp.concatenate([held[j, 2 * pair], held[j, 2 * pair + 1]], axis=1)
+            term = jnp.dot(normed[:, j * depth : (j + 1) * depth], w, preferred_element_type=f32)
+            acc = term if acc is None else acc + term
+        return acc.astype(jnp.bfloat16)
+
+    def halo_kv():
+        return pltpu.make_async_remote_copy(
+            kv.at[pl.ds(rows, WINDOW)], kv.at[pl.ds(0, WINDOW)], halo_send.at[0], halo_recv.at[0],
+            device_id={"sp": up}, device_id_type=MESH_ID,
+        )
+
+    def halo_pool(g):
+        return pltpu.make_async_remote_copy(
+            pool_ext.at[g, pl.ds(rows, TILE)], pool_ext.at[g, pl.ds(0, TILE)],
+            halo_send.at[1 + g], halo_recv.at[1 + g],
+            device_id={"sp": up}, device_id_type=MESH_ID,
+        )
+
+    def first_zero(store):
+        @pl.when(me == 0)
+        def _():
+            store()
+
+    def project_kv():
+        kv[pl.ds(WINDOW, rows), :] = project(0)
+
+        @pl.when(has_up)
+        def _():
+            halo_kv().start()
+
+        def zero():
+            kv[pl.ds(0, WINDOW), :] = jnp.zeros((WINDOW, kv.shape[1]), kv.dtype)
+
+        first_zero(zero)
+
+    def project_q(g):
+        proj[g] = project(1 + g)
+
+    kv_cols = wk.shape[1]
+    kv_heads = kv_cols // HEAD_SIZE
+    group = wq.shape[1] // HEAD_SIZE // kv_heads
+
+    def project_pool(g):
+        pool_ext[g, pl.ds(TILE, rows), :] = project(1 + kv_heads + g)
+
+        @pl.when(has_up)
+        def _():
+            halo_pool(g).start()
+
+        def zero():
+            pool_ext[g, pl.ds(0, TILE), :] = jnp.zeros((TILE, POOL_CH), pool_ext.dtype)
+
+        first_zero(zero)
+
+    def kv_arrived():
+        @pl.when(has_down)
+        def _():
+            halo_kv().wait_recv()
+
+    def attend(b):
+        base = b * WINDOW
+        lane = lax.broadcasted_iota(jnp.int32, (WINDOW, LANES), 1)
+        logs = jnp.zeros((WINDOW, LANES), f32)
+        i_pos = lax.broadcasted_iota(jnp.int32, (WINDOW, 2 * WINDOW), 0)
+        k_pos = lax.broadcasted_iota(jnp.int32, (WINDOW, 2 * WINDOW), 1)
+        allowed = (k_pos > i_pos) & (k_pos <= i_pos + WINDOW)
+        allowed = allowed & (k_pos + (me * rows + base - WINDOW) >= 0)
+        for g in range(kv_heads):
+            band = kv[pl.ds(base, 2 * WINDOW), :]
+            keys = band[:, g * HEAD_SIZE : (g + 1) * HEAD_SIZE]
+            vals = band[:, kv_cols + g * HEAD_SIZE : kv_cols + (g + 1) * HEAD_SIZE]
+            q = proj[g, pl.ds(base, WINDOW), :]
+            q = jnp.concatenate([q[:, h * HEAD_SIZE : (h + 1) * HEAD_SIZE] for h in range(group)], axis=0)
+            scores = lax.dot_general(q, keys, (((1,), (1,)), ((), ())), preferred_element_type=f32)
+            probs = []
+            for h in range(group):
+                head = g * group + h
+                sink = sinks[c * kv_heads * group + head]
+                sc = jnp.where(allowed, scores[h * WINDOW : (h + 1) * WINDOW] * HEAD_SIZE**-0.5, -jnp.inf)
+                top = jnp.maximum(jnp.max(sc, axis=-1, keepdims=True), sink)
+                w = jnp.exp(sc - top)
+                total = jnp.sum(w, axis=-1, keepdims=True) + jnp.exp(sink - top)
+                probs.append((w * (1.0 / total)).astype(jnp.bfloat16))
+                logs = jnp.where(lane == head, top + jnp.log(total), logs)
+            res = jnp.dot(jnp.concatenate(probs, axis=0), vals, preferred_element_type=f32)
+            res = jnp.concatenate([res[h * WINDOW : (h + 1) * WINDOW] for h in range(group)], axis=1)
+            mixed[g, pl.ds(base, WINDOW), :] = res.astype(jnp.bfloat16)
+        log_out[:, pl.ds(base, WINDOW)] = jnp.transpose(logs)[: kv_heads * group]
+
+    def pool(g):
+        @pl.when(has_down)
+        def _():
+            halo_pool(g).wait_recv()
+
+        index = c * groups + g
+        run = pool_ext[g].astype(f32)
+        own = run[TILE:]
+        trailing = jnp.zeros_like(run)
+        span_here = jnp.int32(0)
+        reach = 1
+        for at, span in enumerate(POOL_SPANS):
+            while reach < span:
+                run = run + pltpu.roll(run, reach, 0)
+                reach *= 2
+            trailing = jnp.where(index == at, run, trailing)
+            span_here = jnp.where(index == at, span, span_here)
+        pos = me * rows + lax.broadcasted_iota(jnp.int32, (rows, 1), 0)
+        count = jnp.minimum(pos + 1, span_here).astype(f32)
+        centred = (trailing[TILE:] / count - own).astype(jnp.bfloat16)
+        product = jnp.dot(centred, mix_own[g], preferred_element_type=f32)
+        mixed[kv_heads + g] = (product * pool_gain[index]).astype(jnp.bfloat16)
+
+    n_pairs = out_tiles // 2
+
+    def sum_hop(slot):
+        return pltpu.make_async_remote_copy(
+            sent.at[slot], got.at[slot], sum_send.at[slot], sum_recv.at[slot],
+            device_id={"tp": 1 - c}, device_id_type=MESH_ID,
+        )
+
+    def out_project(j, pair):
+        slot = j * n_pairs + pair
+        acc = None
+        for side in range(2):
+            first = n_in + 4 * pair + side
+            w = jnp.concatenate([held[j, first], held[j, first + 2]], axis=1)
+            parts = mixed.shape[0] // 2
+            a = jnp.concatenate([mixed[side * parts + i] for i in range(parts)], axis=1)
+            term = jnp.dot(a, w, preferred_element_type=f32)
+            acc = term if acc is None else acc + term
+        low, high = acc[:half], acc[half:]
+        mine[slot] = jnp.where(c == 0, low, high)
+        sent[slot] = jnp.where(c == 0, high, low)
+        sum_hop(slot).start()
+
+    def finish(j, pair):
+        slot = j * n_pairs + pair
+        sum_hop(slot).wait()
+        wide = 2 * LANES
+        cols = pl.ds(pl.multiple_of(slot * wide, wide), wide)
+        out[:, cols] = (mine[slot] + got[slot]).astype(jnp.bfloat16)
+
+    tasks = {}
+
+    def ready(block):
+        return (block // 3) * (n - 1) + n - 2
+
+    def at(t, task, *args):
+        tasks.setdefault(min(t, len(slots) - 1), []).append((task, args))
+
+    at(-1, norm_all)
+    at(ready(1), project_kv)
+    for g in range(kv_heads):
+        at(ready(2 * g + 3), project_q, g)
+    last = ready(2 * kv_heads + 1) + 1
+    at(last, kv_arrived)
+    for b in range(rows // WINDOW):
+        at(last + b // 2, attend, b)
+    for g in range(groups):
+        at(ready(2 * (1 + kv_heads + g) + 1), project_pool, g)
+    for g in range(groups):
+        at(ready(2 * (kv_heads + groups) + 1) + (g + 1) // 2, pool, g)
+    base_slot = ready(n_in - 1) + 1
+    for pair in range(n_pairs):
+        at(base_slot, out_project, me, pair)
+    for k in range(n - 1):
+        for pair in range(n_pairs):
+            when = ((n_in + 4 * pair + 3) // 3) * (n - 1) + k
+            at(max(when, base_slot), out_project, shard[k], pair)
+
+    total_slots = len(slots)
+    for t in range(-1, total_slots + 2):
+        if 0 <= t < total_slots:
+            z_step(t)
+        if 0 <= t - 1 < total_slots:
+            x_step(t - 1)
+        if 0 <= t - 2 < total_slots:
+            y_step(t - 2)
+        here = t if t < 0 else t - 2
+        if t in (0, 1):
+            continue
+        for task, args in tasks.pop(here, ()):
+            task(*args)
+    for j in [me] + shard:
+        for pair in range(n_pairs):
+            finish(j, pair)
+
+    for s in range(steps):
+        own_send(s, finish=True)
+    for s, k in slots:
+        way, more = onward(shard[k])
+
+        @pl.when(more)
+        def _():
+            z_hop(s, shard[k], way).wait_send()
+
+        x_hop(s, shard[k]).wait_send()
+        y_hop(s, shard[k]).wait_send()
+
+    @pl.when(has_up)
+    def _():
+        halo_kv().wait_send()
+        for g in range(groups):
+            halo_pool(g).wait_send()
+
+
+def fused_local(
+    n,
+    tokens,
+    norm_gain,
+    query_weight,
+    key_matrix,
+    value_matrix,
+    pool_in_weight,
+    head_sink_logit,
+    pool_mix,
+    pool_gain,
+    attn_out_weight,
+    pool_out_weight,
+):
+    _, half, width = tokens.shape
+    rows = 2 * half
+    depth, q_cols = query_weight.shape
+    kv_cols = key_matrix.shape[1]
+    pool_cols = pool_in_weight.shape[1]
+    heads = q_cols // HEAD_SIZE
+    kv_heads = kv_cols // HEAD_SIZE
+    groups = pool_cols // POOL_CH
+    n_in = (q_cols + 2 * kv_cols + pool_cols) // LANES
+    n_blocks = n_in + 2 * attn_out_weight.shape[1] // LANES
+    steps = n_blocks // 3
+    pieces = n * attn_out_weight.shape[1] // (2 * LANES)
+    bf16, f32 = jnp.bfloat16, jnp.float32
+    dma = pltpu.SemaphoreType.DMA
+    hbm = pl.BlockSpec(memory_space=pl.ANY)
+    vmem = pl.BlockSpec(memory_space=pltpu.VMEM)
+    smem = pl.BlockSpec(memory_space=pltpu.SMEM)
+    mixed, logs = pl.pallas_call(
+        functools.partial(layer_kernel, n),
+        out_shape=(
+            jax.ShapeDtypeStruct((half, width), bf16),
+            jax.ShapeDtypeStruct((heads, rows), f32),
+        ),
+        in_specs=[smem, hbm, vmem, hbm, hbm, hbm, hbm, hbm, vmem, hbm, hbm],
+        out_specs=(vmem, vmem),
+        scratch_shapes=[
+            pltpu.VMEM((n, n_blocks, depth, LANES), bf16),
+            pltpu.VMEM((rows, width), bf16),
+            pltpu.VMEM((rows, width), bf16),
+            pltpu.VMEM((kv_heads, rows, 2 * LANES), bf16),
+            pltpu.VMEM((WINDOW + rows, 2 * kv_cols), bf16),
+            pltpu.VMEM((groups, TILE + rows, POOL_CH), bf16),
+            pltpu.VMEM((kv_heads + groups, rows, 2 * LANES), bf16),
+            pltpu.VMEM((groups, POOL_CH, POOL_CH), bf16),
+            pltpu.VMEM((pieces, half, 2 * LANES), f32),
+            pltpu.VMEM((pieces, half, 2 * LANES), f32),
+            pltpu.VMEM((pieces, half, 2 * LANES), f32),
+            dma((2, steps, n)),
+            dma((steps, n)),
+            dma((steps, n)),
+            dma((steps, n)),
+            dma((steps, n)),
+            dma((steps, n)),
+            dma((n_blocks,)),
+            dma((4,)),
+            dma((1 + groups,)),
+            dma((1 + groups,)),
+            dma((pieces,)),
+            dma((pieces,)),
+        ],
+        compiler_params=pltpu.CompilerParams(
+            collective_id=0, has_side_effects=True, vmem_limit_bytes=60 * 1024 * 1024
+        ),
+    )(
+        head_sink_logit,
+        tokens[0],
+        norm_gain.reshape(1, width),
+        query_weight,
+        key_matrix,
+        value_matrix,
+        pool_in_weight,
+        pool_mix,
+        pool_gain.reshape(-1, 1, POOL_CH),
+        attn_out_weight,
+        pool_out_weight,
+    )
+    return mixed[None], logs[None]
+
+
+def fits(mesh, tokens, query_weight, key_matrix, pool_in_weight, attn_out_weight):
+    n, f, c = mesh.shape["sp"], mesh.shape["fs"], mesh.shape["tp"]
+    depth = query_weight.shape[0] // n
+    rows = tokens.shape[1] // n
+    q_cols, kv_cols, pool_cols = (w.shape[1] // c for w in (query_weight, key_matrix, pool_in_weight))
+    tiles = attn_out_weight.shape[1] // n // LANES
+    blocks = (q_cols + 2 * kv_cols + pool_cols) // LANES + 2 * tiles
+    return (
+        2 <= n <= 4
+        and f == 4
+        and c == 2
+        and tokens.shape[0] == f
+        and rows % WINDOW == 0
+        and kv_cols == LANES
+        and q_cols == 2 * LANES * (kv_cols // HEAD_SIZE)
+        and pool_cols == q_cols
+        and POOL_CH == 2 * LANES
+        and attn_out_weight.shape[1] % (n * 2 * LANES) == 0
+        and attn_out_weight.shape[0] // c == depth
+        and depth % LANES == 0
+        and blocks % 3 == 0
+    )
+
+
 def solution(mesh):
     in_specs = (
         P("fs", ("sp", "tp"), None),
@@ -182,4 +688,11 @@
         P("tp", "sp"),
     )
     out_specs = (P("fs", ("sp", "tp"), None), P("fs", "tp", "sp"))
-    return jax.shard_map(local, mesh=mesh, in_specs=in_specs, out_specs=out_specs, check_vma=False)
+
+    def step(*args):
+        fused = fits(mesh, args[0], args[2], args[3], args[5], args[9])
+        body = functools.partial(fused_local, mesh.shape["sp"]) if fused else local
+        mapped = jax.shard_map(body, mesh=mesh, in_specs=in_specs, out_specs=out_specs, check_vma=False)
+        return mapped(*args)
+
+    return step

time: 244 us -> 96.7 us (0.40)
  waiting for transfers between devices: 134 us -> 0 us
  Pallas kernels: 0 us -> 92.9 us
  blocking collectives: 41 us -> 0 us
  matrix products: 24.4 us -> 0 us
  between operations: 14.6 us -> 0.65 us
  other arithmetic: 12.1 us -> 0 us
  starting transfers between devices: 8.09 us -> 0 us
  local copies, waits for them, and re-layouts: 8.64 us -> 2.92 us
    all_gather x5 -> x0, waiting for transfers between devices: 121 us -> none  [the longest x1 39.8 us: local(): lax.all_gather(attn_out_weight, 'sp', axis=1, tiled=True)]
    pallas_call x0 -> x1, Pallas kernels: none -> 92.9 us  [fused_local(): pl.pallas_call(functools.partial(layer_kernel, n), out_shape=(jax.ShapeDt...]
    all_gather x2 -> x0, blocking collectives: 41 us -> none  [the longest x1 23.4 us: local(): lax.all_gather(value_matrix, 'sp', axis=0, tiled=True)]
    dot_general x9 -> x0, matrix products: 24.4 us -> none  [the longest x4 9.63 us: local(): jnp.dot(normed, weight, preferred_element_type=jnp.float32)]
    reduce_scatter x1 -> x0, waiting for transfers between devices: 10.3 us -> none  [local(): lax.psum_scatter(jnp.dot(attn_part, half_attn, preferred_element_type=jnp...]
    ppermute x3 -> x0, starting transfers between devices: 7.87 us -> none  [passed_along(): return lax.ppermute(shard, axis, pairs)]
    concatenate x8 -> x0, local copies, waits for them, and re-layouts: 3.68 us -> none  [banded(): jnp.concatenate([table[:rows].reshape(blocks, WINDOW, width), table[WINDO...]
    reduce_sum x3 -> x0, other arithmetic: 3.31 us -> none  [the longest x1 2.24 us: local(): jnp.mean(values_f * values_f, axis=-1, keepdims=True) + EPSILON]
  transfers between devices with their start and end apart: 9 -> 0, of which waited for: 6 -> 0; matrix products, arithmetic and copies ran while one was open for 15% -> 0% of each run, Pallas kernels for 0% -> 0%
where the time goes in v1:
time: 96.7 us; the launch traced here: 96.5 us
  Pallas kernels  92.9 us (96%)
  local copies, waits for them, and re-layouts  2.92 us (3%)
    pallas_call x1, Pallas kernels, fused_local(): pl.pallas_call(functools.partial(layer_kernel, n), out_shape=(jax.ShapeDt...  92.9 us
    unnamed x4, local copies, waits for them, and re-layouts  2.92 us

profile of v1, /device:TPU:0, one launch (start us, length us, event | category | flops | bytes accessed | tf_op | source)
XLA Modules:
  0.0 96.5 jit_solution(8837154063204757410)
XLA Ops:
  0.6 92.9 %shard_map.122 = (bf16[256,2048]{1,0:T(8,128)(2,1)}, f32[8,512]{1,0:T(8,128)}) custom-call(f32[16]{0:T(128)} %sinks.1, bf16[256,2048]{1,0:T(8,128)(2,1)} %bitcast.5, f32[1,2048]{1,0:T(1,128)} %bitcast.8, bf16[512,512]{1,0:T(8,128)(2,1)} %wq.1, bf16[512,128]{1,0:T(8,128)(2,1)} %wk.1, bf16[512,128]{1,0:T(8,128)(2,1)} %wv.1, bf16[512,512]{1,0:T(8,128)(2,1)} %wp.1, ...), custom_call_target="tpu_custom_call" | custom-call | tf_op jit(solution)/shard_map/pallas_call | solution.py:600
  93.6 0.0 copy-start
  93.6 2.3 %copy.15 = bf16[1,256,2048]{2,1,0:T(8,128)(2,1)} copy(bf16[1,256,2048]{2,1,0:T(8,128)(2,1)} %bitcast.6) | data formatting | bytes 2097152
  95.9 0.0 copy-done
  95.9 0.6 copy.16
Async XLA Ops:
  93.6 2.3 %copy-start = (f32[8,512]{1,0:T(8,128)S(1)}, f32[8,512]{1,0:T(8,128)}, u32[]{:S(2)}) copy-start(f32[8,512]{1,0:T(8,128)} %get-tuple-element.5) | copy-start | bytes 49156

commit v2 on v1

--- a/solution.py
+++ b/solution.py
@@ -173,6 +173,8 @@
 
 LANES = 128
 TILE = 16
+X_LAG, Y_LAG, LEAD = 2, 4, 2
+CUTS, FAR_LAG = 1, 1
 MESH_ID = pl.DeviceIdType.MESH
 
 
@@ -233,7 +235,7 @@
     n_in = (wq.shape[1] + wk.shape[1] + wv.shape[1] + wp.shape[1]) // LANES
     out_tiles = wao.shape[1] // LANES
     n_blocks = n_in + 2 * out_tiles
-    steps = n_blocks // 3
+    steps = n_blocks // 3 * CUTS
     sources = [wk, wv] + [wq.at[:, pl.ds(i * LANES, LANES)] for i in range(wq.shape[1] // LANES)]
     sources += [wp.at[:, pl.ds(i * LANES, LANES)] for i in range(wp.shape[1] // LANES)]
     for i in range(out_tiles):
@@ -282,7 +284,8 @@
     tok_send.start()
 
     def hop(s, j, part, send, recv, to):
-        block = held.at[j, 3 * s + part]
+        size = depth // CUTS
+        block = held.at[j, 3 * (s // CUTS) + part, pl.ds(s % CUTS * size, size)]
         return pltpu.make_async_remote_copy(
             block, block, send, recv.at[s, j], device_id=to, device_id_type=MESH_ID
         )
@@ -312,13 +315,18 @@
             cp.wait_send() if finish else cp.start()
 
     slots = [(s, k) for s in range(steps) for k in range(n - 1)]
+    slots.sort(key=lambda slot: (slot[0] + FAR_LAG * slot[1], slot))
     shard = [nearest(n, k, me) for k in range(n - 1)]
 
     def z_step(t):
         s, k = slots[t]
         j = shard[k]
-        if k == 0 and s + 1 < steps:
-            own_send(s + 1)
+        if k == 0 and s + LEAD < steps:
+
+            @pl.when(has_up & has_down)
+            def _():
+                own_send(s + LEAD)
+
         z_hop(s, j, 0).wait_recv()
         way, more = onward(j)
 
@@ -339,8 +347,16 @@
 
     for i in range(n_blocks):
         load(i).wait()
-        if i % 3 == 2 and i // 3 == 0:
-            own_send(0)
+        if i % 3 == 2:
+            for s in range(i // 3 * CUTS, (i // 3 + 1) * CUTS):
+                if s < LEAD:
+                    own_send(s)
+                else:
+
+                    @pl.when(jnp.logical_not(has_up & has_down))
+                    def _():
+                        own_send(s)
+
 
     def norm_rows(r, size):
         v = tok[pl.ds(r, size), :].astype(f32)
@@ -505,7 +521,7 @@
     tasks = {}
 
     def ready(block):
-        return (block // 3) * (n - 1) + n - 2
+        return slots.index((block // 3 * CUTS + CUTS - 1, n - 2))
 
     def at(t, task, *args):
         tasks.setdefault(min(t, len(slots) - 1), []).append((task, args))
@@ -523,29 +539,36 @@
     for g in range(groups):
         at(ready(2 * (kv_heads + groups) + 1) + (g + 1) // 2, pool, g)
     base_slot = ready(n_in - 1) + 1
+    order = []
     for pair in range(n_pairs):
         at(base_slot, out_project, me, pair)
+        order.append((base_slot, me, pair))
     for k in range(n - 1):
         for pair in range(n_pairs):
-            when = ((n_in + 4 * pair + 3) // 3) * (n - 1) + k
+            when = slots.index(((n_in + 4 * pair + 3) // 3 * CUTS + CUTS - 1, k))
             at(max(when, base_slot), out_project, shard[k], pair)
-
+            order.append((max(when, base_slot), shard[k], pair))
+
+    late = []
+    for when, j, pair in order:
+        if when + 2 < len(slots) - 1:
+            at(when + 2, finish, j, pair)
+        else:
+            late.append((j, pair))
     total_slots = len(slots)
-    for t in range(-1, total_slots + 2):
-        if 0 <= t < total_slots:
+    for task, args in tasks.pop(-1, ()):
+        task(*args)
+    for t in range(total_slots + Y_LAG):
+        if t < total_slots:
             z_step(t)
-        if 0 <= t - 1 < total_slots:
-            x_step(t - 1)
-        if 0 <= t - 2 < total_slots:
-            y_step(t - 2)
-        here = t if t < 0 else t - 2
-        if t in (0, 1):
-            continue
-        for task, args in tasks.pop(here, ()):
-            task(*args)
-    for j in [me] + shard:
-        for pair in range(n_pairs):
-            finish(j, pair)
+        if 0 <= t - X_LAG < total_slots:
+            x_step(t - X_LAG)
+        if t >= Y_LAG:
+            y_step(t - Y_LAG)
+            for task, args in tasks.pop(t - Y_LAG, ()):
+                task(*args)
+    for j, pair in late:
+        finish(j, pair)
 
     for s in range(steps):
         own_send(s, finish=True)
@@ -590,7 +613,7 @@
     groups = pool_cols // POOL_CH
     n_in = (q_cols + 2 * kv_cols + pool_cols) // LANES
     n_blocks = n_in + 2 * attn_out_weight.shape[1] // LANES
-    steps = n_blocks // 3
+    steps = n_blocks // 3 * CUTS
     pieces = n * attn_out_weight.shape[1] // (2 * LANES)
     bf16, f32 = jnp.bfloat16, jnp.float32
     dma = pltpu.SemaphoreType.DMA

time: 96.7 us -> 83.5 us (0.86)
  the two profiles are of different devices: /device:TPU:0 before, /device:TPU:25 now
where the time goes in v2:
time: 83.5 us; the launch traced here: 83.3 us
  Pallas kernels  79.7 us (95%)
  local copies, waits for them, and re-layouts  2.92 us (3%)
    pallas_call x1, Pallas kernels, fused_local(): pl.pallas_call(functools.partial(layer_kernel, n), out_shape=(jax.ShapeDt...  79.7 us
    unnamed x4, local copies, waits for them, and re-layouts  2.92 us

profile of v2, /device:TPU:25, one launch (start us, length us, event | category | flops | bytes accessed | tf_op | source)
XLA Modules:
  0.0 83.3 jit_solution(1108748148361619173)
XLA Ops:
  0.6 79.7 %shard_map.122 = (bf16[256,2048]{1,0:T(8,128)(2,1)}, f32[8,512]{1,0:T(8,128)}) custom-call(f32[16]{0:T(128)} %sinks.1, bf16[256,2048]{1,0:T(8,128)(2,1)} %bitcast.5, f32[1,2048]{1,0:T(1,128)} %bitcast.8, bf16[512,512]{1,0:T(8,128)(2,1)} %wq.1, bf16[512,128]{1,0:T(8,128)(2,1)} %wk.1, bf16[512,128]{1,0:T(8,128)(2,1)} %wv.1, bf16[512,512]{1,0:T(8,128)(2,1)} %wp.1, ...), custom_call_target="tpu_custom_call" | custom-call | tf_op jit(solution)/shard_map/pallas_call | solution.py:623
  80.3 0.0 copy-start
  80.3 2.3 %copy.15 = bf16[1,256,2048]{2,1,0:T(8,128)(2,1)} copy(bf16[1,256,2048]{2,1,0:T(8,128)(2,1)} %bitcast.6) | data formatting | bytes 2097152
  82.7 0.0 copy-done
  82.7 0.6 copy.16
Async XLA Ops:
  80.3 2.3 %copy-start = (f32[8,512]{1,0:T(8,128)S(1)}, f32[8,512]{1,0:T(8,128)}, u32[]{:S(2)}) copy-start(f32[8,512]{1,0:T(8,128)} %get-tuple-element.5) | copy-start | bytes 49156

commit v3 on v2

--- a/solution.py
+++ b/solution.py
@@ -173,8 +173,8 @@
 
 LANES = 128
 TILE = 16
-X_LAG, Y_LAG, LEAD = 2, 4, 2
-CUTS, FAR_LAG = 1, 1
+X_LAG, Y_LAG, LEAD = 2, 6, 2
+CUTS, FAR_LAG = 1, 0
 MESH_ID = pl.DeviceIdType.MESH
 
 
@@ -336,10 +336,19 @@
 
         x_hop(s, j).start()
 
+        @pl.when(jnp.logical_not(relays))
+        def _():
+            y_hop(s, j).start()
+
+
     def x_step(t):
         s, k = slots[t]
         hop(s, shard[k], x_part, x_send.at[s, shard[k]], x_recv, {"fs": beside}).wait_recv()
-        y_hop(s, shard[k]).start()
+
+        @pl.when(relays)
+        def _():
+            y_hop(s, shard[k]).start()
+
 
     def y_step(t):
         s, k = slots[t]
@@ -556,11 +565,12 @@
         else:
             late.append((j, pair))
     total_slots = len(slots)
-    for task, args in tasks.pop(-1, ()):
-        task(*args)
     for t in range(total_slots + Y_LAG):
         if t < total_slots:
             z_step(t)
+        if t == X_LAG - 1:
+            for task, args in tasks.pop(-1, ()):
+                task(*args)
         if 0 <= t - X_LAG < total_slots:
             x_step(t - X_LAG)
         if t >= Y_LAG:

time: 83.5 us -> 81.8 us (0.980)
  the two profiles are of different devices: /device:TPU:25 before, /device:TPU:0 now
where the time goes in v3:
time: 81.8 us; the launch traced here: 80.6 us
  Pallas kernels  77 us (94%)
  local copies, waits for them, and re-layouts  2.92 us (4%)
    pallas_call x1, Pallas kernels, fused_local(): pl.pallas_call(functools.partial(layer_kernel, n), out_shape=(jax.ShapeDt...  77 us
    unnamed x4, local copies, waits for them, and re-layouts  2.92 us

profile of v3, /device:TPU:0, one launch (start us, length us, event | category | flops | bytes accessed | tf_op | source)
XLA Modules:
  0.0 80.6 jit_solution(5251085472356125292)
XLA Ops:
  0.6 77.0 %shard_map.122 = (bf16[256,2048]{1,0:T(8,128)(2,1)}, f32[8,512]{1,0:T(8,128)}) custom-call(f32[16]{0:T(128)} %sinks.1, bf16[256,2048]{1,0:T(8,128)(2,1)} %bitcast.5, f32[1,2048]{1,0:T(1,128)} %bitcast.8, bf16[512,512]{1,0:T(8,128)(2,1)} %wq.1, bf16[512,128]{1,0:T(8,128)(2,1)} %wk.1, bf16[512,128]{1,0:T(8,128)(2,1)} %wv.1, bf16[512,512]{1,0:T(8,128)(2,1)} %wp.1, ...), custom_call_target="tpu_custom_call" | custom-call | tf_op jit(solution)/shard_map/pallas_call | solution.py:633
  77.6 0.0 copy-start
  77.6 2.3 %copy.15 = bf16[1,256,2048]{2,1,0:T(8,128)(2,1)} copy(bf16[1,256,2048]{2,1,0:T(8,128)(2,1)} %bitcast.6) | data formatting | bytes 2097152
  80.0 0.0 copy-done
  80.0 0.6 copy.16
Async XLA Ops:
  77.6 2.3 %copy-start = (f32[8,512]{1,0:T(8,128)S(1)}, f32[8,512]{1,0:T(8,128)}, u32[]{:S(2)}) copy-start(f32[8,512]{1,0:T(8,128)} %get-tuple-element.5) | copy-start | bytes 49156

commit v4 on v3

--- a/solution.py
+++ b/solution.py
@@ -173,8 +173,8 @@
 
 LANES = 128
 TILE = 16
-X_LAG, Y_LAG, LEAD = 2, 6, 2
-CUTS, FAR_LAG = 1, 0
+X_LAG, Y_LAG, LEAD = 2,6,1
+CUTS, FAR_LAG = 1,0
 MESH_ID = pl.DeviceIdType.MESH
 
 

time: 81.8 us -> 79.4 us (0.971)
  Pallas kernels: 77 us -> 74.3 us
    pallas_call x1, Pallas kernels: 77 us -> 74.3 us  [fused_local(): pl.pallas_call(functools.partial(layer_kernel, n), out_shape=(jax.ShapeDt...]
where the time goes in v4:
time: 79.4 us; the launch traced here: 77.9 us
  Pallas kernels  74.3 us (94%)
  local copies, waits for them, and re-layouts  2.92 us (4%)
    pallas_call x1, Pallas kernels, fused_local(): pl.pallas_call(functools.partial(layer_kernel, n), out_shape=(jax.ShapeDt...  74.3 us
    unnamed x4, local copies, waits for them, and re-layouts  2.92 us

profile of v4, /device:TPU:0, one launch (start us, length us, event | category | flops | bytes accessed | tf_op | source)
XLA Modules:
  0.0 77.9 jit_solution(1119003590243579174)
XLA Ops:
  0.6 74.3 %shard_map.122 = (bf16[256,2048]{1,0:T(8,128)(2,1)}, f32[8,512]{1,0:T(8,128)}) custom-call(f32[16]{0:T(128)} %sinks.1, bf16[256,2048]{1,0:T(8,128)(2,1)} %bitcast.5, f32[1,2048]{1,0:T(1,128)} %bitcast.8, bf16[512,512]{1,0:T(8,128)(2,1)} %wq.1, bf16[512,128]{1,0:T(8,128)(2,1)} %wk.1, bf16[512,128]{1,0:T(8,128)(2,1)} %wv.1, bf16[512,512]{1,0:T(8,128)(2,1)} %wp.1, ...), custom_call_target="tpu_custom_call" | custom-call | tf_op jit(solution)/shard_map/pallas_call | solution.py:633
  75.0 0.0 copy-start
  75.0 2.3 %copy.15 = bf16[1,256,2048]{2,1,0:T(8,128)(2,1)} copy(bf16[1,256,2048]{2,1,0:T(8,128)(2,1)} %bitcast.6) | data formatting | bytes 2097152
  77.3 0.0 copy-done
  77.3 0.6 copy.16
Async XLA Ops:
  75.0 2.3 %copy-start = (f32[8,512]{1,0:T(8,128)S(1)}, f32[8,512]{1,0:T(8,128)}, u32[]{:S(2)}) copy-start(f32[8,512]{1,0:T(8,128)} %get-tuple-element.5) | copy-start | bytes 49156
